TPU v7x, 32 devices: a whole 2x2x4 slice. The times are simulated.
32 devices in a mesh: sp: 8 (over z, x), tp: 4 (over y, core).
Axes of the slice: x: 2, y: 2, z: 4, core: 2. Of those that a mesh axis runs over, the one named last changes fastest.
Arguments:
- residual: bfloat16 [4096, 2048], P('sp'), may hold values from -80 to 80
- queries: bfloat16 [4096, 1024], P('sp', 'tp'), may hold values from -260 to 260
- keys: bfloat16 [4096, 512], P('sp', 'tp'), may hold values from -7 to 7
- values: bfloat16 [4096, 512], P('sp', 'tp'), may hold values from -12 to 12
- documents: int32 [4096], P('sp'), may hold values from 0 to 3, never falling along the last dimension, each value on 1 to 3072 neighbouring positions
- sinks: float32 [16], P('tp'), may hold values from 1 to 6
- out_weight: bfloat16 [1024, 2048], P('tp'), may hold values from -0.5 to 0.5
- norm_gain: float32 [2048], replicated, may hold values from 0.1 to 1.9
- gate_weight: bfloat16 [2048, 5632], P('sp', 'tp'), may hold values from -0.125 to 0.125
- up_weight: bfloat16 [2048, 5632], P('sp', 'tp'), may hold values from -0.125 to 0.125
- down_weight: bfloat16 [2048, 5632], P('sp', 'tp'), may hold values from -0.078125 to 0.078125
Outputs:
- mixed: bfloat16 [4096, 2048], P('sp', 'tp')
Inputs may be any that keep to these rules, and one draw needn't show every extreme that they name: `documents`: document numbers never fall along the positions; a document holds at most 3072 positions.
All inputs are finite; a program needn't handle non-finite values.
Results may differ from a plain program's by a relative error of at most 0.01.
Values may be sent and summed in bfloat16 or wider, within the bound.
A program may use at most 64 MiB of HBM per device.

v0:
```python
import jax
import jax.numpy as jnp
from jax import lax
from jax.sharding import PartitionSpec as P

HEAD_DIM = 64
WINDOW = 128
GROUP = 2
neg_big = -1e30
norm_eps = 1e-05


def from_behind(shard, axis, by):
    length = lax.axis_size(axis)
    pairs = [(i, i + by) for i in range(length) if 0 <= i + by < length]
    return lax.ppermute(shard, axis, pairs)


def attend(queries, keys, values, documents, sinks, tail_keys, tail_values, tail_docs, offset):
    rows_here = queries.shape[0]
    block_count = rows_here // WINDOW
    kv_here = keys.shape[1] // HEAD_DIM
    q_blocks = queries.reshape(block_count, WINDOW, kv_here, GROUP, HEAD_DIM)
    k_blocks = keys.reshape(block_count, WINDOW, kv_here, HEAD_DIM)
    v_blocks = values.reshape(block_count, WINDOW, kv_here, HEAD_DIM)
    k_prev = jnp.concatenate(
        [tail_keys.reshape(1, WINDOW, kv_here, HEAD_DIM), k_blocks[:-1]], axis=0
    )
    v_prev = jnp.concatenate(
        [tail_values.reshape(1, WINDOW, kv_here, HEAD_DIM), v_blocks[:-1]], axis=0
    )
    k_band = jnp.concatenate([k_prev, k_blocks], axis=1)
    v_band = jnp.concatenate([v_prev, v_blocks], axis=1)
    doc_own = documents.astype(jnp.float32).reshape(block_count, WINDOW)
    doc_prev = jnp.concatenate(
        [tail_docs.astype(jnp.float32).reshape(1, WINDOW), doc_own[:-1]], axis=0
    )
    doc_band = jnp.concatenate([doc_prev, doc_own], axis=1)
    row_idx = jnp.arange(WINDOW, dtype=jnp.int32)
    col_idx = jnp.arange(2 * WINDOW, dtype=jnp.int32)
    first = offset + jnp.arange(block_count, dtype=jnp.int32) * WINDOW
    q_pos = first[:, None] + row_idx[None, :]
    k_pos = first[:, None] - WINDOW + col_idx[None, :]
    distance = q_pos[:, :, None] - k_pos[:, None, :]
    visible = (
        (distance >= 0)
        & (distance < WINDOW)
        & (k_pos[:, None, :] >= 0)
        & (doc_own[:, :, None] == doc_band[:, None, :])
    )
    scores = jnp.einsum(
        "nikgd,njkd->nkgij", q_blocks, k_band, preferred_element_type=jnp.float32
    ) * HEAD_DIM ** (-0.5)
    scores = jnp.where(visible[:, None, None], scores, neg_big)
    sink_logit = sinks.reshape(1, kv_here, GROUP, 1, 1)
    row_max = jnp.maximum(scores.max(-1, keepdims=True), sink_logit)
    expo = jnp.where(visible[:, None, None], jnp.exp(scores - row_max), 0.0)
    denom_sum = expo.sum(-1, keepdims=True) + jnp.exp(sink_logit - row_max)
    weights = (expo / denom_sum).astype(jnp.bfloat16)
    mixed = jnp.einsum("nkgij,njkd->nikgd", weights, v_band, preferred_element_type=jnp.float32)
    return mixed.reshape(rows_here, kv_here * GROUP * HEAD_DIM).astype(jnp.bfloat16)


def on_device(
    residual,
    queries,
    keys,
    values,
    documents,
    sinks,
    out_weight,
    norm_gain,
    gate_weight,
    up_weight,
    down_weight,
):
    rows_here = queries.shape[0]
    offset = lax.axis_index("sp") * rows_here
    doc_tail = documents[rows_here - WINDOW :].astype(jnp.bfloat16)
    tail_keys, tail_values, tail_docs = from_behind(
        (keys[rows_here - WINDOW :], values[rows_here - WINDOW :], doc_tail), "sp", 1
    )
    attended = attend(
        queries, keys, values, documents, sinks, tail_keys, tail_values, tail_docs, offset
    )
    model_width = residual.shape[1]
    col_count = model_width // lax.axis_size("tp")
    col_first = lax.axis_index("tp") * col_count
    full_term = jnp.dot(attended, out_weight, preferred_element_type=jnp.float32)
    projected = lax.psum(full_term.astype(jnp.bfloat16), "tp").astype(jnp.float32)
    after_full = (residual.astype(jnp.float32) + projected).astype(jnp.bfloat16)
    after_f = after_full.astype(jnp.float32)
    inv_rms = lax.rsqrt(jnp.mean(after_f * after_f, axis=1, keepdims=True) + norm_eps)
    normed = (after_f * inv_rms * norm_gain[None, :]).astype(jnp.bfloat16)
    after = lax.dynamic_slice_in_dim(after_full, col_first, col_count, 1)
    gate_act = jnp.dot(
        normed,
        lax.all_gather(gate_weight, "sp", axis=0, tiled=True),
        preferred_element_type=jnp.float32,
    )
    up_act = jnp.dot(
        normed,
        lax.all_gather(up_weight, "sp", axis=0, tiled=True),
        preferred_element_type=jnp.float32,
    )
    down_full = lax.all_gather(down_weight, "sp", axis=0, tiled=True)
    hidden = (jax.nn.silu(gate_act) * up_act).astype(jnp.bfloat16)
    summed = lax.psum_scatter(
        lax.dot_general(
            down_full, hidden, (((1,), (1,)), ((), ())), preferred_element_type=jnp.float32
        ).astype(jnp.bfloat16),
        "tp",
        scatter_dimension=0,
        tiled=True,
    ).astype(jnp.float32)
    return (after.astype(jnp.float32) + summed.T).astype(jnp.bfloat16)


def solution(mesh):
    return jax.shard_map(
        on_device,
        mesh=mesh,
        in_specs=(
            P("sp", None),
            P("sp", "tp"),
            P("sp", "tp"),
            P("sp", "tp"),
            P("sp"),
            P("tp"),
            P("tp", None),
            P(),
            P("sp", "tp"),
            P("sp", "tp"),
            P("sp", "tp"),
        ),
        out_specs=P("sp", "tp"),
        check_vma=False,
    )
```

profile of v0, /device:TPU:0, one launch (start us, length us, event | category | flops | bytes accessed | tf_op | source)
XLA Modules:
  0.0 367.5 jit_solution(8054649888373592953)
XLA Ops:
  7.4 0.0 all-reduce.2.cloned.1.call-start
  7.4 0.8 fusion.34
  8.2 4.9 %collective-permute-start.1 = (bf16[128]{0:T(256)(128)(2,1)S(1)}, bf16[128]{0:T(256)(128)(2,1)S(1)}, u32[]{:S(2)}, u32[]{:S(2)}) collective-permute-start(bf16[128]{0:T(256)(128)(2,1)S(1)} %slice.39), channel_id=1, source_target_pairs={{0,4},{4,8},{8,12},{12,16},{16,20},{20,24},{24,28},{1,5},{5,9},{9,... | collective-permute-start | bytes 776 | tf_op jit(solution)/shard_map/ppermute | solution.py:16
  13.1 0.8 slice.42
  13.9 3.4 collective-permute-start.2
  17.3 1.4 slice.36
  18.7 4.0 %collective-permute-start = (bf16[128,128]{1,0:T(8,128)(2,1)}, bf16[128,128]{1,0:T(8,128)(2,1)}, u32[]{:S(2)}, u32[]{:S(2)}) collective-permute-start(bf16[128,128]{1,0:T(8,128)(2,1)} %slice.36), channel_id=1, source_target_pairs={{0,4},{4,8},{8,12},{12,16},{16,20},{20,24},{24,28},{1,5},{5,9},{9,... | collective-permute-start | bytes 98312 | tf_op jit(solution)/shard_map/ppermute | solution.py:16
  22.7 0.1 iota_add_fusion
  22.7 0.1 broadcast_compare_fusion
  22.8 1.0 reshape.148
  23.9 1.0 reshape.146
  24.9 0.1 iota_add_fusion.1
  25.0 2.0 reshape.149
  27.0 0.1 reshape.147
  27.1 0.8 copy.23
  27.9 0.1 copy.25
  28.1 0.1 max.18
  28.2 0.1 reshape.145
  28.3 0.8 copy.18
  29.1 0.1 copy.20
  29.2 0.6 fusion.17
  29.8 0.7 copy.21
  30.5 1.6 fusion.5
  32.2 0.1 broadcast_maximum_fusion
  32.3 0.5 fusion.6
  32.8 0.1 exponential_add_fusion
  32.9 0.9 copy.16
  33.8 0.7 fusion.7
  34.5 0.2 copy.29
  34.7 2.1 convolution_convert_fusion
  36.8 0.0 all-reduce.2.cloned.1.call-update
  36.8 0.0 all-gather.4.cloned.1.call-start
  36.9 0.5 all-gather.4.cloned.1.call-update
  37.4 0.0 all-gather.6.cloned.1.call-start
  37.4 0.5 all-gather.6.cloned.1.call-update
  38.0 0.0 all-gather.8.cloned.1.call-start
  38.0 0.5 all-gather.8.cloned.1.call-update
  38.6 0.2 reduce-scatter.2.cloned.1.call-start
  38.8 48.3 %all-reduce.2.cloned.1.call-done = bf16[512,2048]{1,0:T(8,128)(2,1)} async-done(((bf16[512,2048]{1,0:T(8,128)(2,1)}), bf16[512,2048]{1,0:T(8,128)(2,1)}) %all-reduce.2.cloned.1.call-update) | async-done | bytes 2097168 | tf_op jit(solution)/shard_map/psum | solution.py:90
  87.1 3.2 fusion
  90.3 40.1 %all-gather.4.cloned.1.call-done = bf16[2048,1408]{1,0:T(8,128)(2,1)} async-done(((bf16[256,1408]{1,0:T(8,128)(2,1)}), bf16[2048,1408]{1,0:T(8,128)(2,1)}) %all-gather.4.cloned.1.call-update) | async-done | bytes 5767184 | tf_op jit(solution)/shard_map/all_gather | solution.py:98
  130.4 7.6 %fusion.11 = f32[512,1408]{1,0:T(8,128)} fusion(bf16[2048,1408]{1,0:T(8,128)(2,1)} %all-gather.4.cloned.1.call-done, bf16[512,2048]{1,0:T(8,128)(2,1)S(1)} %get-tuple-element.6, f32[2048]{0:T(1024)S(1)} %copy-done.2, f32[512]{0:T(512)S(1)} %add_rsqrt_fusion), kind=kOutput, calls=%fused_computation.22 | convolution fusion | flops 2956984320 | bytes 10758144 | tf_op jit(solution)/shard_map/dot_general | solution.py:96
  138.0 84.7 %all-gather.6.cloned.1.call-done = bf16[2048,1408]{1,0:T(8,128)(2,1)} async-done(((bf16[256,1408]{1,0:T(8,128)(2,1)}), bf16[2048,1408]{1,0:T(8,128)(2,1)}) %all-gather.6.cloned.1.call-update) | async-done | bytes 5767184 | tf_op jit(solution)/shard_map/all_gather | solution.py:103
  222.7 92.4 %all-gather.8.cloned.1.call-done = bf16[2048,1408]{1,0:T(8,128)(2,1)} async-done(((bf16[256,1408]{1,0:T(8,128)(2,1)}), bf16[2048,1408]{1,0:T(8,128)(2,1)}) %all-gather.8.cloned.1.call-update) | async-done | bytes 5767184 | tf_op jit(solution)/shard_map/all_gather | solution.py:106
  315.1 13.4 %fusion.4 = bf16[2048,512]{0,1:T(8,128)(2,1)} fusion(bf16[2048,1408]{1,0:T(8,128)(2,1)} %all-gather.8.cloned.1.call-done, bf16[2048,1408]{1,0:T(8,128)(2,1)} %all-gather.6.cloned.1.call-done, f32[512,1408]{1,0:T(8,128)} %fusion.11, bf16[512,2048]{1,0:T(8,128)(2,1)S(1)} %get-tuple-element.6, f32[2048]{0:T(1024)S(1)} %copy-done.2, f32[512]{0:T(512)S(1)} %add_rsqrt_fusion), kind=kOutput, calls=%fused_computation.10 | convolution fusion | flops 5915148288 | bytes 18622464 | tf_op jit(solution)/shard_map/dot_general | solution.py:109
  328.5 0.0 reduce-scatter.2.cloned.1.call-update
  328.5 29.5 %reduce-scatter.2.cloned.1.call-done = bf16[512,512]{0,1:T(8,128)(2,1)} async-done(((bf16[2048,512]{0,1:T(8,128)(2,1)}), bf16[512,512]{0,1:T(8,128)(2,1)}) %reduce-scatter.2.cloned.1.call-update) | async-done | bytes 524304 | tf_op jit(solution)/shard_map/reduce_scatter | solution.py:108
  358.0 2.0 fusion.8
  (21 shorter events, 0.1 us)
Async XLA Ops:
  7.4 27.3 %copy-start = (bf16[256,2048]{1,0:T(8,128)(2,1)S(1)}, bf16[256,2048]{1,0:T(8,128)(2,1)}, u32[]{:S(2)}) copy-start(bf16[256,2048]{1,0:T(8,128)(2,1)} %param.17) | copy-start | bytes 3145732
  7.4 19.6 %slice-start = ((bf16[512,128]{1,0:T(8,128)(2,1)}), bf16[384,128]{1,0:T(8,128)(2,1)S(1)}, s32[]{:S(2)}) async-start(bf16[512,128]{1,0:T(8,128)(2,1)} %param.13), calls=%async_computation.6 | async-start | bytes 196608 | tf_op jit(solution)/shard_map/slice | solution.py:27
  7.4 20.8 %slice-start.1 = ((bf16[512,128]{1,0:T(8,128)(2,1)}), bf16[384,128]{1,0:T(8,128)(2,1)S(1)}, s32[]{:S(2)}) async-start(bf16[512,128]{1,0:T(8,128)(2,1)} %param.14), calls=%async_computation.7 | async-start | bytes 196608 | tf_op jit(solution)/shard_map/slice | solution.py:30
  7.4 20.7 %copy-start.3 = (f32[4]{0:T(128)S(1)}, f32[4]{0:T(128)}, u32[]{:S(2)}) copy-start(f32[4]{0:T(128)} %param.16) | copy-start | bytes 52
  7.4 79.7 %all-reduce.2.cloned.1.call-start = ((), (), s32[]{:S(2)}) async-start(), calls=%async_computation.1 | async-start | bytes 4194304 | tf_op jit(solution)/shard_map/psum | solution.py:90
  8.2 21.0 %collective-permute-start.1 = (bf16[128]{0:T(256)(128)(2,1)S(1)}, bf16[128]{0:T(256)(128)(2,1)S(1)}, u32[]{:S(2)}, u32[]{:S(2)}) collective-permute-start(bf16[128]{0:T(256)(128)(2,1)S(1)} %slice.39), channel_id=1, source_target_pairs={{0,4},{4,8},{8,12},{12,16},{16,20},{20,24},{24,28},{1,5},{5,9},{9,... | collective-permute-start | bytes 776 | tf_op jit(solution)/shard_map/ppermute | solution.py:16
  13.9 16.0 %collective-permute-start.2 = (bf16[128,128]{1,0:T(8,128)(2,1)S(1)}, bf16[128,128]{1,0:T(8,128)(2,1)S(1)}, u32[]{:S(2)}, u32[]{:S(2)}) collective-permute-start(bf16[128,128]{1,0:T(8,128)(2,1)S(1)} %slice.42), channel_id=1, source_target_pairs={{0,4},{4,8},{8,12},{12,16},{16,20},{20,24},{24,28},{1,5},{5,9},{9,... | collective-permute-start | bytes 98312 | tf_op jit(solution)/shard_map/ppermute | solution.py:16
  18.7 14.2 %collective-permute-start = (bf16[128,128]{1,0:T(8,128)(2,1)}, bf16[128,128]{1,0:T(8,128)(2,1)}, u32[]{:S(2)}, u32[]{:S(2)}) collective-permute-start(bf16[128,128]{1,0:T(8,128)(2,1)} %slice.36), channel_id=1, source_target_pairs={{0,4},{4,8},{8,12},{12,16},{16,20},{20,24},{24,28},{1,5},{5,9},{9,... | collective-permute-start | bytes 98312 | tf_op jit(solution)/shard_map/ppermute | solution.py:16
  32.2 1.6 copy-start.1
  36.8 93.5 %all-gather.4.cloned.1.call-start = ((), (), s32[]{:S(2)}) async-start(), calls=%async_computation.2 | async-start | bytes 6488064 | tf_op jit(solution)/shard_map/all_gather | solution.py:98
  37.4 185.3 %all-gather.6.cloned.1.call-start = ((), (), s32[]{:S(2)}) async-start(), calls=%async_computation.3 | async-start | bytes 6488064 | tf_op jit(solution)/shard_map/all_gather | solution.py:103
  38.0 277.1 %all-gather.8.cloned.1.call-start = ((), (), s32[]{:S(2)}) async-start(), calls=%async_computation.4 | async-start | bytes 6488064 | tf_op jit(solution)/shard_map/all_gather | solution.py:106
  38.6 91.8 %copy-start.2 = (f32[2048]{0:T(1024)S(1)}, f32[2048]{0:T(1024)}, u32[]{:S(2)}) copy-start(f32[2048]{0:T(1024)} %param.18) | copy-start | bytes 24580
  38.6 319.4 %reduce-scatter.2.cloned.1.call-start = ((), (), s32[]{:S(2)}) async-start(), calls=%async_computation.5 | async-start | bytes 2621440 | tf_op jit(solution)/shard_map/reduce_scatter | solution.py:108
Sparse Core Ops, SparseCore 0:
  36.9 50.1 all-reduce.1
  328.6 29.2 reduce-scatter.1
Sparse Core Ops, SparseCore 1:
  39.5 90.8 all-gather.3
  132.4 90.2 all-gather.5
  224.8 90.2 all-gather.7
where the time goes:
time: 368 us
  waiting for transfers between devices  296 us (80%)
  matrix products  25.5 us (7%)
  between operations  15.2 us (4%)
  starting transfers between devices  12.7 us (3%)
  local copies, waits for them, and re-layouts  10.2 us (3%)
  other arithmetic  7.52 us (2%)
    all_gather x1, waiting for transfers between devices, on_device(): down_full = lax.all_gather(down_weight, 'sp', axis=0, tiled=True)  92.4 us
    all_gather x1, waiting for transfers between devices, on_device(): lax.all_gather(up_weight, 'sp', axis=0, tiled=True)  84.7 us
    psum x1, waiting for transfers between devices, on_device(): lax.psum(full_term.astype(jnp.bfloat16), 'tp').astype(jnp.float32)  48.3 us
    all_gather x1, waiting for transfers between devices, on_device(): lax.all_gather(gate_weight, 'sp', axis=0, tiled=True)  40.1 us
    reduce_scatter x1, waiting for transfers between devices, on_device(): lax.psum_scatter(lax.dot_general(down_full, hidden, (((1,), (1,)), ((), (...  29.5 us
    dot_general x1, matrix products, on_device(): lax.dot_general(down_full, hidden, (((1,), (1,)), ((), ())), preferred_el...  13.4 us
    ppermute x3, starting transfers between devices, from_behind(): return lax.ppermute(shard, axis, pairs)  12.3 us
    dot_general x1, matrix products, on_device(): jnp.dot(normed, lax.all_gather(gate_weight, 'sp', axis=0, tiled=True), pr...  7.64 us
  transfers between devices with their start and end apart: 8, of which 5 were waited for; matrix products, arithmetic and copies ran while one was open for 6% of the time, Pallas kernels for 0%

commit v1 on v0

--- a/solution.py
+++ b/solution.py
@@ -103,7 +103,12 @@
         lax.all_gather(up_weight, "sp", axis=0, tiled=True),
         preferred_element_type=jnp.float32,
     )
-    down_full = lax.all_gather(down_weight, "sp", axis=0, tiled=True)
+    ring = [down_weight]
+    for hop in range(7):
+        ring.append(lax.ppermute(ring[-1], "sp", [(dev, (dev + 1) % 8) for dev in range(8)]))
+    down_full = jnp.roll(
+        jnp.concatenate(ring[::-1], axis=0), (lax.axis_index("sp") + 1) * ring[0].shape[0], axis=0
+    )
     hidden = (jax.nn.silu(gate_act) * up_act).astype(jnp.bfloat16)
     summed = lax.psum_scatter(
         lax.dot_general(

time: 368 us -> 357 us (0.970)
  waiting for transfers between devices: 296 us -> 257 us
  local copies, waits for them, and re-layouts: 10.2 us -> 36.5 us
    ppermute x0 -> x7, waiting for transfers between devices: none -> 209 us  [on_device(): lax.ppermute(ring[-1], 'sp', [(dev, (dev + 1) % 8) for dev in range(8)])]
    all_gather x1 -> x0, waiting for transfers between devices: 92.4 us -> none  [on_device(): down_full = lax.all_gather(down_weight, 'sp', axis=0, tiled=True)]
    all_gather x1, waiting for transfers between devices: 84.7 us -> 16.2 us  [on_device(): lax.all_gather(up_weight, 'sp', axis=0, tiled=True)]
    psum x1, waiting for transfers between devices: 48.3 us -> 0.01 us  [on_device(): lax.psum(full_term.astype(jnp.bfloat16), 'tp').astype(jnp.float32)]
    all_gather x1, waiting for transfers between devices: 40.1 us -> 0.01 us  [on_device(): lax.all_gather(gate_weight, 'sp', axis=0, tiled=True)]
    unnamed x8 -> x43, local copies, waits for them, and re-layouts: 0.02 us -> 22.9 us
  transfers between devices with their start and end apart: 8 -> 14, of which waited for: 5 -> 9; matrix products, arithmetic and copies ran while one was open for 6% -> 13% of each run, Pallas kernels for 0% -> 0%
where the time goes in v1:
time: 357 us; the launch traced here: 356 us
  waiting for transfers between devices  257 us (72%)
  local copies, waits for them, and re-layouts  36.5 us (10%)
  matrix products  26.3 us (7%)
  between operations  15.1 us (4%)
  starting transfers between devices  13.4 us (4%)
  other arithmetic  7.62 us (2%)
    ppermute x7, waiting for transfers between devices, on_device(): lax.ppermute(ring[-1], 'sp', [(dev, (dev + 1) % 8) for dev in range(8)])  209 us
    reduce_scatter x1, waiting for transfers between devices, on_device(): lax.psum_scatter(lax.dot_general(down_full, hidden, (((1,), (1,)), ((), (...  30.9 us
    unnamed x43, local copies, waits for them, and re-layouts  22.9 us
    all_gather x1, waiting for transfers between devices, on_device(): lax.all_gather(up_weight, 'sp', axis=0, tiled=True)  16.2 us
    dot_general x1, matrix products, on_device(): lax.dot_general(down_full, hidden, (((1,), (1,)), ((), ())), preferred_el...  13.3 us
    ppermute x3, starting transfers between devices, from_behind(): return lax.ppermute(shard, axis, pairs)  12.3 us
    dot_general x1, matrix products, on_device(): jnp.dot(normed, lax.all_gather(gate_weight, 'sp', axis=0, tiled=True), pr...  7.77 us
  transfers between devices with their start and end apart: 14, of which 9 were waited for; matrix products, arithmetic and copies ran while one was open for 13% of the time, Pallas kernels for 0%

profile of v1, /device:TPU:0, one launch (start us, length us, event | category | flops | bytes accessed | tf_op | source)
XLA Modules:
  0.0 355.8 jit_solution(9829766244546412125)
XLA Ops:
  8.2 4.9 %collective-permute-start.1 = (bf16[128]{0:T(256)(128)(2,1)S(1)}, bf16[128]{0:T(256)(128)(2,1)S(1)}, u32[]{:S(2)}, u32[]{:S(2)}) collective-permute-start(bf16[128]{0:T(256)(128)(2,1)S(1)} %slice.39), channel_id=1, source_target_pairs={{0,4},{4,8},{8,12},{12,16},{16,20},{20,24},{24,28},{1,5},{5,9},{9,... | collective-permute-start | bytes 776 | tf_op jit(solution)/shard_map/ppermute | solution.py:16
  13.8 3.4 collective-permute-start.2
  17.3 1.4 slice.36
  18.6 4.0 %collective-permute-start = (bf16[128,128]{1,0:T(8,128)(2,1)}, bf16[128,128]{1,0:T(8,128)(2,1)}, u32[]{:S(2)}, u32[]{:S(2)}) collective-permute-start(bf16[128,128]{1,0:T(8,128)(2,1)} %slice.36), channel_id=1, source_target_pairs={{0,4},{4,8},{8,12},{12,16},{16,20},{20,24},{24,28},{1,5},{5,9},{9,... | collective-permute-start | bytes 98312 | tf_op jit(solution)/shard_map/ppermute | solution.py:16
  22.8 1.0 reshape.148
  23.8 0.9 slice.43
  24.7 1.0 reshape.146
  25.8 0.9 slice.37
  26.7 2.0 reshape.149
  32.9 1.6 fusion.9
  35.3 0.9 copy.17
  36.1 1.6 fusion.11
  38.0 2.0 convolution_convert_fusion
  41.3 1.0 collective-permute-start.3
  42.3 26.5 %collective-permute-done.3 = bf16[256,1408]{1,0:T(8,128)(2,1)S(1)} collective-permute-done((bf16[256,1408]{1,0:T(8,128)(2,1)S(1)}, bf16[256,1408]{1,0:T(8,128)(2,1)S(1)}, u32[]{:S(2)}, u32[]{:S(2)}) %collective-permute-start.3) | collective-permute-done | bytes 720928 | tf_op jit(solution)/shard_map/ppermute | solution.py:108
  68.8 0.9 copy-done.3
  69.7 30.1 %collective-permute-done.4 = bf16[256,1408]{1,0:T(8,128)(2,1)S(1)} collective-permute-done((bf16[256,1408]{1,0:T(8,128)(2,1)S(1)}, bf16[256,1408]{1,0:T(8,128)(2,1)S(1)}, u32[]{:S(2)}, u32[]{:S(2)}) %collective-permute-start.4) | collective-permute-done | bytes 720928 | tf_op jit(solution)/shard_map/ppermute | solution.py:108
  99.8 0.9 copy-done.5
  100.7 35.4 %collective-permute-done.5 = bf16[256,1408]{1,0:T(8,128)(2,1)S(1)} collective-permute-done((bf16[256,1408]{1,0:T(8,128)(2,1)S(1)}, bf16[256,1408]{1,0:T(8,128)(2,1)S(1)}, u32[]{:S(2)}, u32[]{:S(2)}) %collective-permute-start.5) | collective-permute-done | bytes 720928 | tf_op jit(solution)/shard_map/ppermute | solution.py:108
  136.1 0.8 copy-done.7
  137.0 35.2 %collective-permute-done.6 = bf16[256,1408]{1,0:T(8,128)(2,1)S(1)} collective-permute-done((bf16[256,1408]{1,0:T(8,128)(2,1)S(1)}, bf16[256,1408]{1,0:T(8,128)(2,1)S(1)}, u32[]{:S(2)}, u32[]{:S(2)}) %collective-permute-start.6) | collective-permute-done | bytes 720928 | tf_op jit(solution)/shard_map/ppermute | solution.py:108
  172.1 0.9 copy-done.9
  173.0 23.6 %collective-permute-done.7 = bf16[256,1408]{1,0:T(8,128)(2,1)S(1)} collective-permute-done((bf16[256,1408]{1,0:T(8,128)(2,1)S(1)}, bf16[256,1408]{1,0:T(8,128)(2,1)S(1)}, u32[]{:S(2)}, u32[]{:S(2)}) %collective-permute-start.7) | collective-permute-done | bytes 720928 | tf_op jit(solution)/shard_map/ppermute | solution.py:108
  196.7 0.9 copy-done.11
  197.6 35.2 %collective-permute-done.8 = bf16[256,1408]{1,0:T(8,128)(2,1)} collective-permute-done((bf16[256,1408]{1,0:T(8,128)(2,1)S(1)}, bf16[256,1408]{1,0:T(8,128)(2,1)}, u32[]{:S(2)}, u32[]{:S(2)}) %collective-permute-start.8) | collective-permute-done | bytes 720928 | tf_op jit(solution)/shard_map/ppermute | solution.py:108
  232.7 3.3 fusion.2
  236.1 22.8 %collective-permute-done.9 = bf16[256,1408]{1,0:T(8,128)(2,1)} collective-permute-done((bf16[256,1408]{1,0:T(8,128)(2,1)}, bf16[256,1408]{1,0:T(8,128)(2,1)}, u32[]{:S(2)}, u32[]{:S(2)}) %collective-permute-start.9) | collective-permute-done | bytes 720928 | tf_op jit(solution)/shard_map/ppermute | solution.py:108
  258.9 2.0 constant_dynamic-update-slice_fusion.15
  260.9 2.1 constant_dynamic-update-slice_fusion.14
  263.0 0.9 constant_dynamic-update-slice_fusion.13
  263.9 0.9 constant_dynamic-update-slice_fusion.12
  264.9 0.9 constant_dynamic-update-slice_fusion.11
  265.8 0.9 constant_dynamic-update-slice_fusion.10
  266.7 0.9 constant_dynamic-update-slice_fusion.9
  267.6 0.9 constant_dynamic-update-slice_fusion.8
  268.5 2.0 constant_dynamic-update-slice_fusion.7
  270.6 2.0 constant_dynamic-update-slice_fusion.6
  272.6 0.9 constant_dynamic-update-slice_fusion.5
  273.5 1.0 constant_dynamic-update-slice_fusion.4
  274.5 1.0 constant_dynamic-update-slice_fusion.3
  275.5 0.9 constant_dynamic-update-slice_fusion.2
  276.4 0.9 constant_dynamic-update-slice_fusion.1
  277.3 0.9 constant_dynamic-update-slice_fusion
  278.2 7.8 %fusion.14 = f32[512,1408]{1,0:T(8,128)} fusion(bf16[2048,1408]{1,0:T(8,128)(2,1)} %all-gather.3.cloned.1.call-done, bf16[512,2048]{1,0:T(8,128)(2,1)S(1)} %get-tuple-element.6, f32[2048]{0:T(1024)S(1)} %copy-done.13, f32[512]{0:T(512)S(1)} %add_rsqrt_fusion), kind=kOutput, calls=%fused_computation.23 | convolution fusion | flops 2956984320 | bytes 10758144 | tf_op jit(solution)/shard_map/dot_general | solution.py:96
  286.0 16.2 %all-gather.5.cloned.1.call-done = bf16[2048,1408]{1,0:T(8,128)(2,1)} async-done(((bf16[256,1408]{1,0:T(8,128)(2,1)}), bf16[2048,1408]{1,0:T(8,128)(2,1)}) %all-gather.5.cloned.1.call-update) | async-done | bytes 5767184 | tf_op jit(solution)/shard_map/all_gather | solution.py:103
  302.2 13.3 %fusion.6 = bf16[2048,512]{0,1:T(8,128)(2,1)} fusion(bf16[4096,1408]{1,0:T(8,128)(2,1)} %constant_dynamic-update-slice_fusion, s32[]{:T(128)S(6)} %select_n.27, bf16[2048,1408]{1,0:T(8,128)(2,1)} %all-gather.5.cloned.1.call-done, f32[512,1408]{1,0:T(8,128)} %fusion.14, bf16[512,2048]{1,0:T(8,128)(2,1)S(1)} %get-tuple-element.6, f32[2048]{0:T(1024)S(1)} %copy-done.13, ...), kind=kOutput, calls=%fused_computation.11 | convolution fusion | flops 5915148288 | bytes 18622468 | tf_op jit(solution)/shard_map/dot_general | solution.py:114
  315.5 30.9 %reduce-scatter.2.cloned.1.call-done = bf16[512,512]{0,1:T(8,128)(2,1)} async-done(((bf16[2048,512]{0,1:T(8,128)(2,1)}), bf16[512,512]{0,1:T(8,128)(2,1)}) %reduce-scatter.2.cloned.1.call-update) | async-done | bytes 524304 | tf_op jit(solution)/shard_map/reduce_scatter | solution.py:113
  346.4 2.0 fusion.12
  (66 shorter events, 8.1 us)
Async XLA Ops:
  7.4 30.6 %copy-start = (bf16[256,2048]{1,0:T(8,128)(2,1)S(1)}, bf16[256,2048]{1,0:T(8,128)(2,1)}, u32[]{:S(2)}) copy-start(bf16[256,2048]{1,0:T(8,128)(2,1)} %param.17) | copy-start | bytes 3145732
  7.4 225.4 %all-reduce.2.cloned.1.call-start = ((), (), s32[]{:S(2)}) async-start(), calls=%async_computation.1 | async-start | bytes 4194304 | tf_op jit(solution)/shard_map/psum | solution.py:90
  8.2 23.4 %collective-permute-start.1 = (bf16[128]{0:T(256)(128)(2,1)S(1)}, bf16[128]{0:T(256)(128)(2,1)S(1)}, u32[]{:S(2)}, u32[]{:S(2)}) collective-permute-start(bf16[128]{0:T(256)(128)(2,1)S(1)} %slice.39), channel_id=1, source_target_pairs={{0,4},{4,8},{8,12},{12,16},{16,20},{20,24},{24,28},{1,5},{5,9},{9,... | collective-permute-start | bytes 776 | tf_op jit(solution)/shard_map/ppermute | solution.py:16
  13.8 18.4 %collective-permute-start.2 = (bf16[128,128]{1,0:T(8,128)(2,1)S(1)}, bf16[128,128]{1,0:T(8,128)(2,1)S(1)}, u32[]{:S(2)}, u32[]{:S(2)}) collective-permute-start(bf16[128,128]{1,0:T(8,128)(2,1)S(1)} %slice.42), channel_id=1, source_target_pairs={{0,4},{4,8},{8,12},{12,16},{16,20},{20,24},{24,28},{1,5},{5,9},{9,... | collective-permute-start | bytes 98312 | tf_op jit(solution)/shard_map/ppermute | solution.py:16
  18.6 16.6 %collective-permute-start = (bf16[128,128]{1,0:T(8,128)(2,1)}, bf16[128,128]{1,0:T(8,128)(2,1)}, u32[]{:S(2)}, u32[]{:S(2)}) collective-permute-start(bf16[128,128]{1,0:T(8,128)(2,1)} %slice.36), channel_id=1, source_target_pairs={{0,4},{4,8},{8,12},{12,16},{16,20},{20,24},{24,28},{1,5},{5,9},{9,... | collective-permute-start | bytes 98312 | tf_op jit(solution)/shard_map/ppermute | solution.py:16
  37.7 3.5 copy-start.1
  40.0 238.2 %all-gather.3.cloned.1.call-start = ((), (), s32[]{:S(2)}) async-start(), calls=%async_computation.2 | async-start | bytes 6488064 | tf_op jit(solution)/shard_map/all_gather | solution.py:98
  40.6 261.6 %all-gather.5.cloned.1.call-start = ((), (), s32[]{:S(2)}) async-start(), calls=%async_computation.3 | async-start | bytes 6488064 | tf_op jit(solution)/shard_map/all_gather | solution.py:103
  41.2 305.1 %reduce-scatter.2.cloned.1.call-start = ((), (), s32[]{:S(2)}) async-start(), calls=%async_computation.4 | async-start | bytes 2621440 | tf_op jit(solution)/shard_map/reduce_scatter | solution.py:113
  41.3 27.5 %collective-permute-start.3 = (bf16[256,1408]{1,0:T(8,128)(2,1)S(1)}, bf16[256,1408]{1,0:T(8,128)(2,1)S(1)}, u32[]{:S(2)}, u32[]{:S(2)}) collective-permute-start(bf16[256,1408]{1,0:T(8,128)(2,1)S(1)} %copy-done.1), channel_id=1, source_target_pairs={{0,4},{4,8},{8,12},{12,16},{16,20},{20,24},{24,28},{28,0},{1,5},{5... | collective-permute-start | bytes 2162696 | tf_op jit(solution)/shard_map/ppermute | solution.py:108
  68.8 0.9 copy-start.3
  69.7 30.1 %collective-permute-start.4 = (bf16[256,1408]{1,0:T(8,128)(2,1)S(1)}, bf16[256,1408]{1,0:T(8,128)(2,1)S(1)}, u32[]{:S(2)}, u32[]{:S(2)}) collective-permute-start(bf16[256,1408]{1,0:T(8,128)(2,1)S(1)} %collective-permute-done.3), channel_id=1, source_target_pairs={{0,4},{4,8},{8,12},{12,16},{16,20},{20,24},{24,28},{28,0},{1,5},{5... | collective-permute-start | bytes 2162696 | tf_op jit(solution)/shard_map/ppermute | solution.py:108
  99.8 0.9 copy-start.5
  100.7 35.4 %collective-permute-start.5 = (bf16[256,1408]{1,0:T(8,128)(2,1)S(1)}, bf16[256,1408]{1,0:T(8,128)(2,1)S(1)}, u32[]{:S(2)}, u32[]{:S(2)}) collective-permute-start(bf16[256,1408]{1,0:T(8,128)(2,1)S(1)} %collective-permute-done.4), channel_id=1, source_target_pairs={{0,4},{4,8},{8,12},{12,16},{16,20},{20,24},{24,28},{28,0},{1,5},{5... | collective-permute-start | bytes 2162696 | tf_op jit(solution)/shard_map/ppermute | solution.py:108
  136.1 0.8 copy-start.7
  137.0 35.2 %collective-permute-start.6 = (bf16[256,1408]{1,0:T(8,128)(2,1)S(1)}, bf16[256,1408]{1,0:T(8,128)(2,1)S(1)}, u32[]{:S(2)}, u32[]{:S(2)}) collective-permute-start(bf16[256,1408]{1,0:T(8,128)(2,1)S(1)} %collective-permute-done.5), channel_id=1, source_target_pairs={{0,4},{4,8},{8,12},{12,16},{16,20},{20,24},{24,28},{28,0},{1,5},{5... | collective-permute-start | bytes 2162696 | tf_op jit(solution)/shard_map/ppermute | solution.py:108
  172.1 0.9 copy-start.9
  173.0 23.7 %collective-permute-start.7 = (bf16[256,1408]{1,0:T(8,128)(2,1)S(1)}, bf16[256,1408]{1,0:T(8,128)(2,1)S(1)}, u32[]{:S(2)}, u32[]{:S(2)}) collective-permute-start(bf16[256,1408]{1,0:T(8,128)(2,1)S(1)} %collective-permute-done.6), channel_id=1, source_target_pairs={{0,4},{4,8},{8,12},{12,16},{16,20},{20,24},{24,28},{28,0},{1,5},{5... | collective-permute-start | bytes 2162696 | tf_op jit(solution)/shard_map/ppermute | solution.py:108
  196.7 0.9 copy-start.11
  197.6 35.2 %collective-permute-start.8 = (bf16[256,1408]{1,0:T(8,128)(2,1)S(1)}, bf16[256,1408]{1,0:T(8,128)(2,1)}, u32[]{:S(2)}, u32[]{:S(2)}) collective-permute-start(bf16[256,1408]{1,0:T(8,128)(2,1)S(1)} %collective-permute-done.7), channel_id=1, source_target_pairs={{0,4},{4,8},{8,12},{12,16},{16,20},{20,24},{24,28},{28,0},{1,5},{5... | collective-permute-start | bytes 2162696 | tf_op jit(solution)/shard_map/ppermute | solution.py:108
  232.7 26.1 %collective-permute-start.9 = (bf16[256,1408]{1,0:T(8,128)(2,1)}, bf16[256,1408]{1,0:T(8,128)(2,1)}, u32[]{:S(2)}, u32[]{:S(2)}) collective-permute-start(bf16[256,1408]{1,0:T(8,128)(2,1)} %collective-permute-done.8), channel_id=1, source_target_pairs={{0,4},{4,8},{8,12},{12,16},{16,20},{20,24},{24,28},{28,0},{1,5},{5... | collective-permute-start | bytes 2162696 | tf_op jit(solution)/shard_map/ppermute | solution.py:108
  232.7 30.3 %copy-start.12 = (bf16[256,1408]{1,0:T(8,128)(2,1)S(1)}, bf16[256,1408]{1,0:T(8,128)(2,1)}, u32[]{:S(2)}) copy-start(bf16[256,1408]{1,0:T(8,128)(2,1)} %copy-done.11) | copy-start | bytes 2162692
  232.7 31.2 %copy-start.10 = (bf16[256,1408]{1,0:T(8,128)(2,1)S(1)}, bf16[256,1408]{1,0:T(8,128)(2,1)}, u32[]{:S(2)}) copy-start(bf16[256,1408]{1,0:T(8,128)(2,1)} %copy-done.9) | copy-start | bytes 2162692
  236.1 28.8 %copy-start.8 = (bf16[256,1408]{1,0:T(8,128)(2,1)S(1)}, bf16[256,1408]{1,0:T(8,128)(2,1)}, u32[]{:S(2)}) copy-start(bf16[256,1408]{1,0:T(8,128)(2,1)} %copy-done.7) | copy-start | bytes 2162692
  236.1 29.7 %copy-start.6 = (bf16[256,1408]{1,0:T(8,128)(2,1)S(1)}, bf16[256,1408]{1,0:T(8,128)(2,1)}, u32[]{:S(2)}) copy-start(bf16[256,1408]{1,0:T(8,128)(2,1)} %copy-done.5) | copy-start | bytes 2162692
  236.1 30.6 %copy-start.4 = (bf16[256,1408]{1,0:T(8,128)(2,1)S(1)}, bf16[256,1408]{1,0:T(8,128)(2,1)}, u32[]{:S(2)}) copy-start(bf16[256,1408]{1,0:T(8,128)(2,1)} %copy-done.3) | copy-start | bytes 2162692
  260.9 6.7 %copy-start.2 = (bf16[256,1408]{1,0:T(8,128)(2,1)S(1)}, bf16[256,1408]{1,0:T(8,128)(2,1)}, u32[]{:S(2)}) copy-start(bf16[256,1408]{1,0:T(8,128)(2,1)} %param.21) | copy-start | bytes 2162692
  272.6 5.6 %copy-start.13 = (f32[2048]{0:T(1024)S(1)}, f32[2048]{0:T(1024)}, u32[]{:S(2)}) copy-start(f32[2048]{0:T(1024)} %param.18) | copy-start | bytes 24580
Sparse Core Ops, SparseCore 0:
  40.2 50.0 all-reduce.1
  315.6 30.6 reduce-scatter.1
Sparse Core Ops, SparseCore 1:
  42.7 132.2 all-gather.2
  177.0 125.1 all-gather.4
